TPU v7x, 32 devices: a whole 2x2x4 slice. The times are simulated.
32 devices in a mesh: ep: 16 (over z, y, x), tp: 2 (over core).
Axes of the slice: x: 2, y: 2, z: 4, core: 2. Of those that a mesh axis runs over, the one named last changes fastest.
Arguments:
- tokens: bfloat16 [512, 2048], P('ep'), may hold values from -6 to 6
- mix_gain: float32 [2048], replicated, may hold values from 0.1 to 1.9
- w_query: bfloat16 [2048, 512], P('ep', 'tp'), may hold values from -0.125 to 0.125
- w_key: bfloat16 [2048, 512], P('ep', 'tp'), may hold values from -0.125 to 0.125
- w_value: bfloat16 [2048, 512], P('ep', 'tp'), may hold values from -0.125 to 0.125
- w_outgate: bfloat16 [2048, 512], P('ep', 'tp'), may hold values from -0.125 to 0.125
- w_igate: bfloat16 [2048, 8], P('ep', 'tp'), may hold values from -0.125 to 0.125
- w_fgate: bfloat16 [2048, 8], P('ep', 'tp'), may hold values from -0.125 to 0.125
- igate_bias: float32 [8], P('tp'), may hold values from -2 to 1
- fgate_bias: float32 [8], P('tp'), may hold values from 0 to 4
- head_gain: float32 [512], P('tp'), may hold values from 0.1 to 1.9
- w_out: bfloat16 [512, 2048], P('tp', 'ep'), may hold values from -0.25 to 0.25
- state_matrix: float32 [512, 8, 64, 64], P('ep', 'tp'), may hold values from -2.4 to 2.4
- state_norm: float32 [512, 8, 64], P('ep', 'tp'), may hold values from -2.4 to 2.4
- state_max: float32 [512, 8], P('ep', 'tp'), may hold values from -4 to 4
- ffn_gain: float32 [2048], replicated, may hold values from 0.1 to 1.9
- w_expert_gate: bfloat16 [16, 2048, 1408], P('ep', None, 'tp'), may hold values from -0.125 to 0.125
- w_expert_up: bfloat16 [16, 2048, 1408], P('ep', None, 'tp'), may hold values from -0.125 to 0.125
- w_expert_down: bfloat16 [16, 1408, 2048], P('ep', 'tp'), may hold values from -0.15625 to 0.15625
- routes: int32 [512, 3], P('ep'), may hold values from 0 to 15, all different within a row; in each aligned block of 32 rows (0 to 31, 32 to 63, ...) at most 12 rows name the same one
- route_weights: float32 [512, 3], P('ep'), may hold values from 0.2 to 1
Outputs:
- mixed: bfloat16 [512, 2048], P('ep')
- new_matrix: float32 [512, 8, 64, 64], P('ep', 'tp')
- new_norm: float32 [512, 8, 64], P('ep', 'tp')
- new_max: float32 [512, 8], P('ep', 'tp')
Inputs may be any that keep to these rules, and one draw needn't show every extreme that they name: `routes`: each row names 3 different experts. Among the rows of one device, no expert is named by more than 12 rows, a bound that some block reaches.
All inputs are finite; a program needn't handle non-finite values.
Results may differ from a plain program's by a relative error of at most 0.017.
Values may be sent and summed in bfloat16 or wider, within the bound.
No kernel may reach another device: no remote copies, remote signals or barrier semaphores. Data moves between devices by JAX's collectives and lax.ppermute only.
A program may use at most 128 MiB of HBM per device.

v0:
```python
import jax
import jax.numpy as jnp
from jax import lax
from jax.sharding import PartitionSpec as P


def rms_scale(values_in, gain_vec):
    widened = values_in.astype(jnp.float32)
    return (
        widened * lax.rsqrt(jnp.mean(widened * widened, axis=-1, keepdims=True) + 1e-06) * gain_vec
    )


def memory_cell(
    query,
    key_row,
    value_row,
    outgate,
    input_pre,
    forget_pre,
    head_gain,
    state_matrix,
    state_norm,
    state_max,
):
    seq_rows, head_count = input_pre.shape
    head_size = query.shape[1] // head_count
    query_heads = query.astype(jnp.float32).reshape(seq_rows, head_count, head_size)
    key_heads = key_row.astype(jnp.float32).reshape(
        seq_rows, head_count, head_size
    ) * head_size ** (-0.5)
    value_heads = value_row.astype(jnp.float32).reshape(seq_rows, head_count, head_size)
    log_forget = jax.nn.log_sigmoid(forget_pre)
    new_max = jnp.maximum(log_forget + state_max, input_pre)
    keep_old = jnp.exp(log_forget + state_max - new_max)
    keep_new = jnp.exp(input_pre - new_max)
    new_matrix = (
        keep_old[:, :, None, None] * state_matrix
        + keep_new[:, :, None, None] * value_heads[:, :, :, None] * key_heads[:, :, None, :]
    )
    new_norm = keep_old[:, :, None] * state_norm + keep_new[:, :, None] * key_heads
    numerator = jnp.einsum(
        "bhvd,bhd->bhv", new_matrix, query_heads, precision=lax.Precision.HIGHEST
    )
    denominator = jnp.sum(new_norm * query_heads, axis=-1)
    cell_read = numerator / jnp.maximum(jnp.abs(denominator), jnp.exp(-new_max))[:, :, None]
    centered = cell_read - jnp.mean(cell_read, axis=-1, keepdims=True)
    variance = jnp.mean(centered * centered, axis=-1, keepdims=True)
    scaled_cell = (centered * lax.rsqrt(variance + 1e-06)).reshape(seq_rows, head_count * head_size)
    cell_out = (scaled_cell * head_gain * jax.nn.sigmoid(outgate.astype(jnp.float32))).astype(
        jnp.bfloat16
    )
    return (cell_out, new_matrix, new_norm, new_max)


def body(
    tokens,
    mix_gain,
    w_query,
    w_key,
    w_value,
    w_outgate,
    w_igate,
    w_fgate,
    igate_bias,
    fgate_bias,
    head_gain,
    w_out,
    state_matrix,
    state_norm,
    state_max,
    ffn_gain,
    w_expert_gate,
    w_expert_up,
    w_expert_down,
    routes,
    route_weights,
):
    seq_rows, width = tokens.shape
    normed = rms_scale(tokens, mix_gain).astype(jnp.bfloat16)
    weight_list = (w_query, w_key, w_value, w_outgate, w_igate, w_fgate)
    spread = lax.all_to_all(normed, "ep", split_axis=1, concat_axis=0, tiled=True)
    joined = jnp.concatenate(weight_list, axis=1)
    summed = lax.psum_scatter(
        jnp.dot(spread, joined, preferred_element_type=jnp.float32),
        "ep",
        scatter_dimension=0,
        tiled=True,
    )
    bounds = [0]
    for weight in weight_list:
        bounds.append(bounds[-1] + weight.shape[1])
    projected = tuple(
        (summed[:, bounds[index] : bounds[index + 1]] for index in range(len(weight_list)))
    )
    query = projected[0].astype(jnp.bfloat16)
    key_row = projected[1].astype(jnp.bfloat16)
    value_row = projected[2].astype(jnp.bfloat16)
    outgate = projected[3].astype(jnp.bfloat16)
    input_pre = projected[4] + igate_bias
    forget_pre = projected[5] + fgate_bias
    cell_out, new_matrix, new_norm, new_max = memory_cell(
        query,
        key_row,
        value_row,
        outgate,
        input_pre,
        forget_pre,
        head_gain,
        state_matrix,
        state_norm,
        state_max,
    )
    partial_out = jnp.dot(
        cell_out,
        lax.all_gather(w_out, "ep", axis=1, tiled=True),
        preferred_element_type=jnp.float32,
    )
    attended = lax.psum(partial_out.astype(jnp.bfloat16), "tp").astype(jnp.float32)
    resid = (tokens.astype(jnp.float32) + attended).astype(jnp.bfloat16)
    normed_two = rms_scale(resid, ffn_gain).astype(jnp.bfloat16)
    ep_count = lax.axis_size("ep")
    local_experts = w_expert_gate.shape[0]
    expert_total = local_experts * ep_count
    top_count = routes.shape[1]
    capacity = max(2, 2 * seq_rows * top_count // expert_total)
    flat_routes = routes.reshape(-1)
    onehot = (flat_routes[:, None] == jnp.arange(expert_total, dtype=jnp.int32)[None, :]).astype(
        jnp.int32
    )
    earlier = jnp.cumsum(onehot, axis=0, dtype=jnp.int32) - onehot
    slots = jnp.sum(onehot * earlier, axis=1, dtype=jnp.int32)
    targets = flat_routes * capacity + slots
    dispatch = (
        targets[:, None] == jnp.arange(expert_total * capacity, dtype=jnp.int32)[None, :]
    ).astype(jnp.bfloat16)
    route_rows = jnp.repeat(normed_two, top_count, axis=0)
    outgoing = jnp.einsum(
        "rs,rd->sd", dispatch, route_rows, preferred_element_type=jnp.float32
    ).astype(jnp.bfloat16)
    outgoing = outgoing.reshape(expert_total, capacity, width)
    received = lax.all_to_all(outgoing, "ep", split_axis=0, concat_axis=0, tiled=True)
    slot_count = received.shape[1]
    regrouped = received.reshape(ep_count, local_experts, slot_count, width)
    gate_pre = jnp.einsum(
        "nxcd,xdf->nxcf", regrouped, w_expert_gate, preferred_element_type=jnp.float32
    )
    up_pre = jnp.einsum(
        "nxcd,xdf->nxcf", regrouped, w_expert_up, preferred_element_type=jnp.float32
    )
    hidden = (jax.nn.silu(gate_pre) * up_pre).astype(jnp.bfloat16)
    partial_down = jnp.einsum(
        "nxcf,xfd->nxcd", hidden, w_expert_down, preferred_element_type=jnp.float32
    )
    expert_sum = lax.psum(partial_down.astype(jnp.bfloat16), "tp")
    finished = expert_sum.reshape(ep_count * local_experts, slot_count, width)
    returned = lax.all_to_all(finished, "ep", split_axis=0, concat_axis=0, tiled=True)
    picked = jnp.dot(
        dispatch,
        returned.reshape(expert_total * capacity, width),
        preferred_element_type=jnp.float32,
    )
    weighted = jnp.sum(
        picked.reshape(seq_rows, top_count, width) * route_weights[:, :, None], axis=1
    )
    mixed = (resid.astype(jnp.float32) + weighted).astype(jnp.bfloat16)
    return (mixed, new_matrix, new_norm, new_max)


def solution(mesh):
    placed = (
        P("ep", None),
        P(),
        P("ep", "tp"),
        P("ep", "tp"),
        P("ep", "tp"),
        P("ep", "tp"),
        P("ep", "tp"),
        P("ep", "tp"),
        P("tp"),
        P("tp"),
        P("tp"),
        P("tp", "ep"),
        P("ep", "tp", None, None),
        P("ep", "tp", None),
        P("ep", "tp"),
        P(),
        P("ep", None, "tp"),
        P("ep", None, "tp"),
        P("ep", "tp", None),
        P("ep", None),
        P("ep", None),
    )
    return jax.shard_map(
        body,
        mesh=mesh,
        in_specs=placed,
        out_specs=(P("ep", None), P("ep", "tp", None, None), P("ep", "tp", None), P("ep", "tp")),
        check_vma=False,
    )
```

profile of v0, /device:TPU:8, one launch (start us, length us, event | category | flops | bytes accessed | tf_op | source)
XLA Modules:
  0.0 342.0 jit_solution(8380659892496630698)
XLA Ops:
  7.2 1.2 fusion.36
  8.4 1.7 copy_bitcast_fusion
  10.1 7.2 %all-to-all-start = ((bf16[32,16,128]{2,0,1:T(8,128)(2,1)}), bf16[32,16,128]{2,0,1:T(8,128)(2,1)S(1)}, u32[]{:S(2)}, u32[]{:S(2)}) async-start(bf16[32,16,128]{2,0,1:T(8,128)(2,1)} %copy_bitcast_fusion), calls=%async_computation | async-start | bytes 262144 | tf_op jit(solution)/shard_map/all_to_all | solution.py:82
  17.3 0.8 copy.58
  18.1 0.8 copy.59
  19.0 1.1 concatenate.3
  20.0 3.9 %all-to-all-done = bf16[32,16,128]{2,0,1:T(8,128)(2,1)S(1)} async-done(((bf16[32,16,128]{2,0,1:T(8,128)(2,1)}), bf16[32,16,128]{2,0,1:T(8,128)(2,1)S(1)}, u32[]{:S(2)}, u32[]{:S(2)}) %all-to-all-start) | async-done | bytes 131104 | tf_op jit(solution)/shard_map/all_to_all | solution.py:82
  23.9 1.9 fusion.62
  25.8 0.7 all-gather.2.cloned.1.call-update
  26.8 0.1 eq.50
  27.0 0.1 reduce_window_sum.11
  27.1 0.2 select_reduce_fusion
  27.3 125.7 %reduce-scatter.2.cloned.1.call-done = f32[32,1032]{1,0:T(8,128)} async-done(((f32[512,1032]{1,0:T(8,128)}), f32[32,1032]{1,0:T(8,128)}) %reduce-scatter.2.cloned.1.call-update) | async-done | bytes 132112 | tf_op jit(solution)/shard_map/reduce_scatter | solution.py:84
  153.0 0.9 convert.9
  154.1 0.1 reshape.171
  154.4 0.9 broadcast_multiply_fusion.3
  155.3 0.8 subtract_exponential_fusion.1
  156.1 0.8 multiply_reduce_fusion.1
  156.9 3.8 %multiply_add_fusion = f32[32,4,64,64]{3,2,1,0:T(8,128)S(1)} fusion(f32[32,4,64,64]{3,2,1,0:T(8,128)} %param.33, f32[32,4,64]{2,1,0:T(4,128)S(1)} %get-tuple-element.30, f32[32,4,64]{2,1,0:T(4,128)S(1)} %get-tuple-element.31, f32[32,4]{1,0:T(8,128)S(1)} %subtract_exponential_fusion.1), kind=kLoop, calls=%fused_computation | loop fusion | flops 1572864 | bytes 4260352 | tf_op jit(solution)/shard_map/add | solution.py:38
  160.7 2.0 copy-done.1
  162.7 3.4 fusion.63
  166.1 0.2 fusion.59
  166.3 0.2 multiply_reduce_fusion
  166.5 0.1 subtract_multiply_fusion
  166.6 0.1 reshape.152
  166.7 39.0 %all-gather.2.cloned.1.call-done = bf16[256,2048]{1,0:T(8,128)(2,1)} async-done(((bf16[256,128]{1,0:T(8,128)(2,1)}), bf16[256,2048]{1,0:T(8,128)(2,1)}) %all-gather.2.cloned.1.call-update) | async-done | bytes 1048592 | tf_op jit(solution)/shard_map/all_gather | solution.py:116
  205.7 2.2 convolution_convert_fusion.1
  207.9 0.5 multiply_add_fusion.3
  208.4 18.1 %all-reduce.3.cloned.1.call-done = bf16[32,2048]{1,0:T(8,128)(2,1)} async-done(((bf16[32,2048]{1,0:T(8,128)(2,1)}), bf16[32,2048]{1,0:T(8,128)(2,1)}) %all-reduce.3.cloned.1.call-update) | async-done | bytes 131088 | tf_op jit(solution)/shard_map/psum | solution.py:119
  226.5 1.1 fusion.40
  227.6 1.0 fusion.42
  228.6 0.2 broadcast_in_dim.2
  228.8 1.1 reshape.153
  229.9 2.4 convolution_convert_fusion
  232.3 2.1 reshape.154
  234.4 33.1 %all_to_all.29 = bf16[16,12,2048]{2,1,0:T(8,128)(2,1)S(1)} all-to-all(bf16[16,12,2048]{2,1,0:T(8,128)(2,1)} %reshape.154), channel_id=1, replica_groups=mesh['ep'=16,'tp'=2] {'ep'}, dimensions={0} | all-to-all | bytes 1572864 | tf_op jit(solution)/shard_map/all_to_all | solution.py:142
  267.5 1.0 copy-done.4
  268.5 3.8 %fusion.9 = f32[16,1,12,704]{3,0,2,1:T(8,128)} fusion(bf16[1,2048,704]{1,2,0:T(8,128)(2,1)} %param.37, bf16[16,12,2048]{2,1,0:T(8,128)(2,1)S(1)} %all_to_all.29), kind=kOutput, calls=%fused_computation.11 | convolution fusion | flops 553648128 | bytes 4210688 | tf_op jit(solution)/shard_map/nxcd,xdf->nxcf/dot_general | solution.py:145
  272.3 5.2 %fusion.6 = bf16[16,12,2048]{2,0,1:T(8,128)(2,1)} fusion(bf16[1,704,2048]{2,1,0:T(8,128)(2,1)S(1)} %copy-done, bf16[1,2048,704]{1,2,0:T(8,128)(2,1)} %param.38, f32[16,1,12,704]{3,0,2,1:T(8,128)} %fusion.9, bf16[16,12,2048]{2,1,0:T(8,128)(2,1)} %copy-done.4), kind=kOutput, calls=%fused_computation.7 | convolution fusion | flops 1108500480 | bytes 7880704 | tf_op jit(solution)/shard_map/nxcf,xfd->nxcd/dot_general | solution.py:152
  277.6 17.9 %all-reduce.5.cloned.1.call-done = bf16[16,12,2048]{2,0,1:T(8,128)(2,1)} async-done(((bf16[16,12,2048]{2,0,1:T(8,128)(2,1)}), bf16[16,12,2048]{2,0,1:T(8,128)(2,1)}) %all-reduce.5.cloned.1.call-update) | async-done | bytes 786448 | tf_op jit(solution)/shard_map/psum | solution.py:155
  295.5 2.6 copy.65
  298.1 7.1 %all-to-all-start.2 = ((bf16[16,12,2048]{2,1,0:T(8,128)(2,1)}), bf16[16,12,2048]{2,1,0:T(8,128)(2,1)}, u32[]{:S(2)}, u32[]{:S(2)}) async-start(bf16[16,12,2048]{2,1,0:T(8,128)(2,1)} %copy.65), calls=%async_computation.3 | async-start | bytes 2097152 | tf_op jit(solution)/shard_map/all_to_all | solution.py:157
  305.2 0.1 reduce_sum.70
  305.4 0.7 copy.66
  306.0 25.1 %all-to-all-done.2 = bf16[16,12,2048]{2,1,0:T(8,128)(2,1)} async-done(((bf16[16,12,2048]{2,1,0:T(8,128)(2,1)}), bf16[16,12,2048]{2,1,0:T(8,128)(2,1)}, u32[]{:S(2)}, u32[]{:S(2)}) %all-to-all-start.2) | async-done | bytes 786464 | tf_op jit(solution)/shard_map/all_to_all | solution.py:157
  331.1 2.1 reshape.169
  333.2 1.5 fusion.18
  334.7 0.7 fusion.43
  (51 shorter events, 0.9 us)
Async XLA Ops:
  7.2 265.2 %copy-start = (bf16[1,704,2048]{2,1,0:T(8,128)(2,1)S(1)}, bf16[1,704,2048]{2,1,0:T(8,128)(2,1)}, u32[]{:S(2)}) copy-start(bf16[1,704,2048]{2,1,0:T(8,128)(2,1)} %param.39) | copy-start | bytes 8650756
  10.1 13.8 %all-to-all-start = ((bf16[32,16,128]{2,0,1:T(8,128)(2,1)}), bf16[32,16,128]{2,0,1:T(8,128)(2,1)S(1)}, u32[]{:S(2)}, u32[]{:S(2)}) async-start(bf16[32,16,128]{2,0,1:T(8,128)(2,1)} %copy_bitcast_fusion), calls=%async_computation | async-start | bytes 262144 | tf_op jit(solution)/shard_map/all_to_all | solution.py:82
  17.3 135.7 %reduce-scatter.2.cloned.1.call-start = ((), (), s32[]{:S(2)}) async-start(), calls=%async_computation.4 | async-start | bytes 2506752 | tf_op jit(solution)/shard_map/reduce_scatter | solution.py:84
  18.9 7.6 %copy-start.13 = (f32[32,4]{0,1:T(4,128)S(1)}, f32[32,4]{0,1:T(4,128)}, u32[]{:S(2)}) copy-start(f32[32,4]{0,1:T(4,128)} %param.35) | copy-start | bytes 1540
  18.9 7.7 %copy-start.7 = (s32[32,3]{0,1:T(4,128)S(1)}, s32[32,3]{0,1:T(4,128)}, u32[]{:S(2)}) copy-start(s32[32,3]{0,1:T(4,128)} %param.40) | copy-start | bytes 1156
  23.9 130.5 %copy-start.10 = (f32[4]{0:T(128)S(1)}, f32[4]{0:T(128)}, u32[]{:S(2)}) copy-start(f32[4]{0:T(128)} %param.30) | copy-start | bytes 52
  23.9 130.5 %copy-start.15 = (f32[4]{0:T(128)S(1)}, f32[4]{0:T(128)}, u32[]{:S(2)}) copy-start(f32[4]{0:T(128)} %param.29) | copy-start | bytes 52
  23.9 132.2 %copy-start.5 = (f32[32,4,64]{2,1,0:T(4,128)S(1)}, f32[32,4,64]{2,1,0:T(4,128)}, u32[]{:S(2)}) copy-start(f32[32,4,64]{2,1,0:T(4,128)} %param.34) | copy-start | bytes 98308
  25.8 179.9 %all-gather.2.cloned.1.call-start = ((), (), s32[]{:S(2)}) async-start(), calls=%async_computation.5 | async-start | bytes 1114112 | tf_op jit(solution)/shard_map/all_gather | solution.py:116
  26.5 200.0 %all-reduce.3.cloned.1.call-start = ((), (), s32[]{:S(2)}) async-start(), calls=%async_computation.6 | async-start | bytes 262144 | tf_op jit(solution)/shard_map/psum | solution.py:119
  27.3 180.6 %copy-start.11 = (s32[96]{0:T(128)}, s32[96]{0:T(128)S(1)}, u32[]{:S(2)}) copy-start(s32[96]{0:T(128)S(1)} %select_reduce_fusion) | copy-start | bytes 1156
  160.7 2.0 copy-start.1
  162.7 43.0 %copy-start.14 = (f32[256]{0:T(256)S(1)}, f32[256]{0:T(256)}, u32[]{:S(2)}) copy-start(f32[256]{0:T(256)} %param.31) | copy-start | bytes 3076
  162.7 63.8 %copy-start.2 = (bf16[32,2048]{1,0:T(8,128)(2,1)S(1)}, bf16[32,2048]{1,0:T(8,128)(2,1)}, u32[]{:S(2)}) copy-start(bf16[32,2048]{1,0:T(8,128)(2,1)} %param.21) | copy-start | bytes 393220
  162.7 64.9 %copy-start.6 = (f32[2048]{0:T(1024)S(1)}, f32[2048]{0:T(1024)}, u32[]{:S(2)}) copy-start(f32[2048]{0:T(1024)} %param.36) | copy-start | bytes 24580
  207.9 87.6 %all-reduce.5.cloned.1.call-start = ((), (), s32[]{:S(2)}) async-start(), calls=%async_computation.7 | async-start | bytes 1572864 | tf_op jit(solution)/shard_map/psum | solution.py:155
  267.5 1.0 copy-start.4
  277.5 27.7 %copy-start.12 = (s32[96]{0:T(128)S(1)}, s32[96]{0:T(128)}, u32[]{:S(2)}) copy-start(s32[96]{0:T(128)} %copy-done.11) | copy-start | bytes 1156
  277.5 27.8 %copy-start.8 = (s32[32,3]{0,1:T(4,128)S(1)}, s32[32,3]{0,1:T(4,128)}, u32[]{:S(2)}) copy-start(s32[32,3]{0,1:T(4,128)} %param.40) | copy-start | bytes 1156
  277.6 55.7 %copy-start.9 = (f32[32,3]{0,1:T(4,128)S(1)}, f32[32,3]{0,1:T(4,128)}, u32[]{:S(2)}) copy-start(f32[32,3]{0,1:T(4,128)} %param.41) | copy-start | bytes 1156
  298.1 36.6 %copy-start.3 = (bf16[32,2048]{1,0:T(8,128)(2,1)S(1)}, bf16[32,2048]{1,0:T(8,128)(2,1)}, u32[]{:S(2)}) copy-start(bf16[32,2048]{1,0:T(8,128)(2,1)} %all-reduce.3.cloned.1.call-done) | copy-start | bytes 393220
  298.1 33.0 %all-to-all-start.2 = ((bf16[16,12,2048]{2,1,0:T(8,128)(2,1)}), bf16[16,12,2048]{2,1,0:T(8,128)(2,1)}, u32[]{:S(2)}, u32[]{:S(2)}) async-start(bf16[16,12,2048]{2,1,0:T(8,128)(2,1)} %copy.65), calls=%async_computation.3 | async-start | bytes 2097152 | tf_op jit(solution)/shard_map/all_to_all | solution.py:157
Sparse Core Ops, SparseCore 0:
  25.9 127.0 reduce-scatter.1
  155.7 49.9 all-gather.1
  208.6 17.9 all-reduce.2
  277.7 17.7 all-reduce.4
where the time goes:
time: 343 us; the launch traced here: 342 us
  waiting for transfers between devices  230 us (67%)
  blocking collectives  33.1 us (10%)
  matrix products  20.2 us (6%)
  local copies, waits for them, and re-layouts  15.4 us (4%)
  starting transfers between devices  14.5 us (4%)
  other arithmetic  14.3 us (4%)
  between operations  14 us (4%)
    reduce_scatter x1, waiting for transfers between devices, body(): lax.psum_scatter(jnp.dot(spread, joined, preferred_element_type=jnp.float...  126 us
    all_gather x1, waiting for transfers between devices, body(): lax.all_gather(w_out, 'ep', axis=1, tiled=True)  39 us
    all_to_all x1, blocking collectives, body(): lax.all_to_all(outgoing, 'ep', split_axis=0, concat_axis=0, tiled=True)  33.1 us
    all_to_all x1, waiting for transfers between devices, body(): lax.all_to_all(finished, 'ep', split_axis=0, concat_axis=0, tiled=True)  25.1 us
    psum x1, waiting for transfers between devices, body(): lax.psum(partial_out.astype(jnp.bfloat16), 'tp').astype(jnp.float32)  18.1 us
    psum x1, waiting for transfers between devices, body(): expert_sum = lax.psum(partial_down.astype(jnp.bfloat16), 'tp')  17.9 us
    all_to_all x1, starting transfers between devices, body(): lax.all_to_all(normed, 'ep', split_axis=1, concat_axis=0, tiled=True)  7.22 us
    all_to_all x1, starting transfers between devices, body(): lax.all_to_all(finished, 'ep', split_axis=0, concat_axis=0, tiled=True)  7.11 us
  transfers between devices with their start and end apart: 6, of which 6 were waited for; matrix products, arithmetic and copies ran while one was open for 5% of the time, Pallas kernels for 0%

commit v1 on v0

--- a/solution.py
+++ b/solution.py
@@ -2,6 +2,28 @@
 import jax.numpy as jnp
 from jax import lax
 from jax.sharding import PartitionSpec as P
+
+
+def seats_all_spread(load, bus_axis, dim_no):
+    far_arr, odd, ready = (lax.axis_size(bus_axis), lax.axis_index(bus_axis), load.shape[dim_no])
+    views = [i * far_arr if src_i == dim_no else i for src_i, i in enumerate(load.shape)]
+    reply = lax.dynamic_update_slice_in_dim(
+        jnp.zeros(views, load.dtype), load, odd * ready, axis=dim_no
+    )
+    z1 = outcome_arr = load
+    for m in range(1, far_arr // 2 + 1):
+        z1 = lax.ppermute(
+            z1, bus_axis, [(src_i, (src_i + 1) % far_arr) for src_i in range(far_arr)]
+        )
+        reply = lax.dynamic_update_slice_in_dim(reply, z1, (odd - m) % far_arr * ready, axis=dim_no)
+        if 2 * m < far_arr:
+            outcome_arr = lax.ppermute(
+                outcome_arr, bus_axis, [(src_i, (src_i - 1) % far_arr) for src_i in range(far_arr)]
+            )
+            reply = lax.dynamic_update_slice_in_dim(
+                reply, outcome_arr, (odd + m) % far_arr * ready, axis=dim_no
+            )
+    return reply
 
 
 def rms_scale(values_in, gain_vec):
@@ -112,9 +134,7 @@
         state_max,
     )
     partial_out = jnp.dot(
-        cell_out,
-        lax.all_gather(w_out, "ep", axis=1, tiled=True),
-        preferred_element_type=jnp.float32,
+        cell_out, seats_all_spread(w_out, "ep", 1), preferred_element_type=jnp.float32
     )
     attended = lax.psum(partial_out.astype(jnp.bfloat16), "tp").astype(jnp.float32)
     resid = (tokens.astype(jnp.float32) + attended).astype(jnp.bfloat16)

time: 343 us -> 304 us (0.89)
  waiting for transfers between devices: 230 us -> 154 us
  starting transfers between devices: 14.5 us -> 41.2 us
  local copies, waits for them, and re-layouts: 15.4 us -> 26.8 us
    reduce_scatter x1, waiting for transfers between devices: 126 us -> 74.9 us  [body(): lax.psum_scatter(jnp.dot(spread, joined, preferred_element_type=jnp.float...]
    all_gather x1 -> x0, waiting for transfers between devices: 39 us -> none  [body(): lax.all_gather(w_out, 'ep', axis=1, tiled=True)]
    ppermute x0 -> x15, starting transfers between devices: none -> 26.7 us  [the longest x7 26.1 us: seats_all_spread(): lax.ppermute(outcome_arr, bus_axis, [(src_i, (src_i - 1) % far_arr) for s...]
    ppermute x0 -> x15, waiting for transfers between devices: none -> 14.8 us  [the longest x8 11.9 us: seats_all_spread(): lax.ppermute(z1, bus_axis, [(src_i, (src_i + 1) % far_arr) for src_i in r...]
    dynamic_update_slice x0 -> x16, local copies, waits for them, and re-layouts: none -> 10.2 us  [the longest x8 5.19 us: seats_all_spread(): lax.dynamic_update_slice_in_dim(reply, z1, (odd - m) % far_arr * ready, a...]
  transfers between devices with their start and end apart: 6 -> 20, of which waited for: 6 -> 17; matrix products, arithmetic and copies ran while one was open for 5% -> 5% of each run, Pallas kernels for 0% -> 0%
where the time goes in v1:
time: 304 us; the launch traced here: 303 us
  waiting for transfers between devices  154 us (51%)
  starting transfers between devices  41.2 us (14%)
  blocking collectives  33.1 us (11%)
  local copies, waits for them, and re-layouts  26.8 us (9%)
  matrix products  20.3 us (7%)
  other arithmetic  14.3 us (5%)
  between operations  14.1 us (5%)
    reduce_scatter x1, waiting for transfers between devices, body(): lax.psum_scatter(jnp.dot(spread, joined, preferred_element_type=jnp.float...  74.9 us
    all_to_all x1, blocking collectives, body(): lax.all_to_all(outgoing, 'ep', split_axis=0, concat_axis=0, tiled=True)  33.1 us
    ppermute x7, starting transfers between devices, seats_all_spread(): lax.ppermute(outcome_arr, bus_axis, [(src_i, (src_i - 1) % far_arr) for s...  26.1 us
    all_to_all x1, waiting for transfers between devices, body(): lax.all_to_all(finished, 'ep', split_axis=0, concat_axis=0, tiled=True)  25.1 us
    psum x1, waiting for transfers between devices, body(): expert_sum = lax.psum(partial_down.astype(jnp.bfloat16), 'tp')  17.9 us
    psum x1, waiting for transfers between devices, body(): lax.psum(partial_out.astype(jnp.bfloat16), 'tp').astype(jnp.float32)  17 us
    ppermute x8, waiting for transfers between devices, seats_all_spread(): lax.ppermute(z1, bus_axis, [(src_i, (src_i + 1) % far_arr) for src_i in r...  11.9 us
    all_to_all x1, starting transfers between devices, body(): lax.all_to_all(normed, 'ep', split_axis=1, concat_axis=0, tiled=True)  7.22 us
  transfers between devices with their start and end apart: 20, of which 17 were waited for; matrix products, arithmetic and copies ran while one was open for 5% of the time, Pallas kernels for 0%

profile of v1, /device:TPU:8, one launch (start us, length us, event | category | flops | bytes accessed | tf_op | source)
XLA Modules:
  0.0 303.3 jit_solution(15579684290840699312)
XLA Ops:
  7.2 1.2 fusion.36
  8.4 1.7 copy_bitcast_fusion
  10.1 7.2 %all-to-all-start = ((bf16[32,16,128]{2,0,1:T(8,128)(2,1)}), bf16[32,16,128]{2,0,1:T(8,128)(2,1)S(1)}, u32[]{:S(2)}, u32[]{:S(2)}) async-start(bf16[32,16,128]{2,0,1:T(8,128)(2,1)} %copy_bitcast_fusion), calls=%async_computation | async-start | bytes 262144 | tf_op jit(solution)/shard_map/all_to_all | solution.py:104
  17.3 0.8 copy.58
  18.1 0.8 copy.59
  18.9 1.1 concatenate.3
  20.0 3.8 %all-to-all-done = bf16[32,16,128]{2,0,1:T(8,128)(2,1)S(1)} async-done(((bf16[32,16,128]{2,0,1:T(8,128)(2,1)}), bf16[32,16,128]{2,0,1:T(8,128)(2,1)S(1)}, u32[]{:S(2)}, u32[]{:S(2)}) %all-to-all-start) | async-done | bytes 131104 | tf_op jit(solution)/shard_map/all_to_all | solution.py:104
  23.9 1.9 fusion.62
  25.8 1.5 collective-permute-start.1
  28.7 1.1 broadcast_in_dim.4
  30.4 3.3 %collective-permute-start.3 = (bf16[256,128]{1,0:T(8,128)(2,1)S(1)}, bf16[256,128]{1,0:T(8,128)(2,1)S(1)}, u32[]{:S(2)}, u32[]{:S(2)}) collective-permute-start(bf16[256,128]{1,0:T(8,128)(2,1)S(1)} %collective-permute-done.1), channel_id=1, source_target_pairs={{0,30},{2,0},{4,2},{6,4},{8,6},{10,8},{12,10},{14,12},{16,14},{18,... | collective-permute-start | bytes 196616 | tf_op jit(solution)/shard_map/ppermute | solution.py:20
  35.0 0.8 collective-permute-done.3
  35.8 4.0 %collective-permute-start.5 = (bf16[256,128]{1,0:T(8,128)(2,1)S(1)}, bf16[256,128]{1,0:T(8,128)(2,1)S(1)}, u32[]{:S(2)}, u32[]{:S(2)}) collective-permute-start(bf16[256,128]{1,0:T(8,128)(2,1)S(1)} %collective-permute-done.3), channel_id=1, source_target_pairs={{0,30},{2,0},{4,2},{6,4},{8,6},{10,8},{12,10},{14,12},{16,14},{18,... | collective-permute-start | bytes 196616 | tf_op jit(solution)/shard_map/ppermute | solution.py:20
  39.9 0.7 constant_dynamic-update-slice_fusion.12
  41.8 4.3 %collective-permute-start.7 = (bf16[256,128]{1,0:T(8,128)(2,1)S(1)}, bf16[256,128]{1,0:T(8,128)(2,1)S(1)}, u32[]{:S(2)}, u32[]{:S(2)}) collective-permute-start(bf16[256,128]{1,0:T(8,128)(2,1)S(1)} %collective-permute-done.5), channel_id=1, source_target_pairs={{0,30},{2,0},{4,2},{6,4},{8,6},{10,8},{12,10},{14,12},{16,14},{18,... | collective-permute-start | bytes 196616 | tf_op jit(solution)/shard_map/ppermute | solution.py:20
  47.8 0.8 collective-permute-done.7
  48.6 4.4 %collective-permute-start.9 = (bf16[256,128]{1,0:T(8,128)(2,1)S(1)}, bf16[256,128]{1,0:T(8,128)(2,1)S(1)}, u32[]{:S(2)}, u32[]{:S(2)}) collective-permute-start(bf16[256,128]{1,0:T(8,128)(2,1)S(1)} %collective-permute-done.7), channel_id=1, source_target_pairs={{0,30},{2,0},{4,2},{6,4},{8,6},{10,8},{12,10},{14,12},{16,14},{18,... | collective-permute-start | bytes 196616 | tf_op jit(solution)/shard_map/ppermute | solution.py:20
  55.2 4.2 %collective-permute-start.11 = (bf16[256,128]{1,0:T(8,128)(2,1)S(1)}, bf16[256,128]{1,0:T(8,128)(2,1)S(1)}, u32[]{:S(2)}, u32[]{:S(2)}) collective-permute-start(bf16[256,128]{1,0:T(8,128)(2,1)S(1)} %collective-permute-done.9), channel_id=1, source_target_pairs={{0,30},{2,0},{4,2},{6,4},{8,6},{10,8},{12,10},{14,12},{16,14},{18,... | collective-permute-start | bytes 196616 | tf_op jit(solution)/shard_map/ppermute | solution.py:20
  61.5 4.4 %collective-permute-start.13 = (bf16[256,128]{1,0:T(8,128)(2,1)S(1)}, bf16[256,128]{1,0:T(8,128)(2,1)S(1)}, u32[]{:S(2)}, u32[]{:S(2)}) collective-permute-start(bf16[256,128]{1,0:T(8,128)(2,1)S(1)} %collective-permute-done.11), channel_id=1, source_target_pairs={{0,30},{2,0},{4,2},{6,4},{8,6},{10,8},{12,10},{14,12},{16,14},{18,... | collective-permute-start | bytes 196616 | tf_op jit(solution)/shard_map/ppermute | solution.py:20
  67.6 5.1 %collective-permute-done.12 = bf16[256,128]{1,0:T(8,128)(2,1)S(1)} collective-permute-done((bf16[256,128]{1,0:T(8,128)(2,1)S(1)}, bf16[256,128]{1,0:T(8,128)(2,1)S(1)}, u32[]{:S(2)}, u32[]{:S(2)}) %collective-permute-start.12) | collective-permute-done | bytes 65568 | tf_op jit(solution)/shard_map/ppermute | solution.py:15
  72.8 0.7 constant_dynamic-update-slice_fusion.2
  74.1 4.8 %collective-permute-done.14 = bf16[256,128]{1,0:T(8,128)(2,1)S(1)} collective-permute-done((bf16[256,128]{1,0:T(8,128)(2,1)S(1)}, bf16[256,128]{1,0:T(8,128)(2,1)S(1)}, u32[]{:S(2)}, u32[]{:S(2)}) %collective-permute-start.14) | collective-permute-done | bytes 65568 | tf_op jit(solution)/shard_map/ppermute | solution.py:15
  79.5 74.9 %reduce-scatter.2.cloned.1.call-done = f32[32,1032]{1,0:T(8,128)} async-done(((f32[512,1032]{1,0:T(8,128)}), f32[32,1032]{1,0:T(8,128)}) %reduce-scatter.2.cloned.1.call-update) | async-done | bytes 132112 | tf_op jit(solution)/shard_map/reduce_scatter | solution.py:106
  154.3 0.9 convert.9
  155.7 0.9 broadcast_multiply_fusion.3
  156.6 0.8 subtract_exponential_fusion.1
  157.4 0.8 multiply_reduce_fusion.1
  158.2 3.8 %multiply_add_fusion = f32[32,4,64,64]{3,2,1,0:T(8,128)S(1)} fusion(f32[32,4,64,64]{3,2,1,0:T(8,128)} %param.33, f32[32,4,64]{2,1,0:T(4,128)S(1)} %get-tuple-element.30, f32[32,4,64]{2,1,0:T(4,128)S(1)} %get-tuple-element.31, f32[32,4]{1,0:T(8,128)S(1)} %subtract_exponential_fusion.1), kind=kLoop, calls=%fused_computation | loop fusion | flops 1572864 | bytes 4260352 | tf_op jit(solution)/shard_map/add | solution.py:60
  162.0 2.0 copy-done.1
  164.0 3.4 %fusion.63 = f32[32,4,1,64]{3,2,1,0:T(1,128)S(1)} fusion(f32[32,4,64,64]{3,2,1,0:T(8,128)S(1)} %multiply_add_fusion, bf16[32,4,64,1]{2,3,1,0:T(2,128)(2,1)S(1)} %reshape.171), kind=kOutput, calls=%fused_computation.100 | convolution fusion | flops 6291456 | bytes 2146304 | tf_op jit(solution)/shard_map/bhvd,bhd->bhv/dot_general | solution.py:64
  168.0 2.2 convolution_convert_fusion.1
  170.8 17.0 %all-reduce.3.cloned.1.call-done = bf16[32,2048]{1,0:T(8,128)(2,1)} async-done(((bf16[32,2048]{1,0:T(8,128)(2,1)}), bf16[32,2048]{1,0:T(8,128)(2,1)}) %all-reduce.3.cloned.1.call-update) | async-done | bytes 131088 | tf_op jit(solution)/shard_map/psum | solution.py:139
  187.8 1.1 fusion.40
  188.9 1.0 fusion.42
  190.1 1.1 reshape.153
  191.2 2.4 convolution_convert_fusion
  193.6 2.1 reshape.154
  195.8 33.1 %all_to_all.29 = bf16[16,12,2048]{2,1,0:T(8,128)(2,1)S(1)} all-to-all(bf16[16,12,2048]{2,1,0:T(8,128)(2,1)} %reshape.154), channel_id=1, replica_groups=mesh['ep'=16,'tp'=2] {'ep'}, dimensions={0} | all-to-all | bytes 1572864 | tf_op jit(solution)/shard_map/all_to_all | solution.py:162
  228.9 1.0 copy-done.4
  229.8 3.8 %fusion.9 = f32[16,1,12,704]{3,0,2,1:T(8,128)} fusion(bf16[1,2048,704]{1,2,0:T(8,128)(2,1)} %param.37, bf16[16,12,2048]{2,1,0:T(8,128)(2,1)S(1)} %all_to_all.29), kind=kOutput, calls=%fused_computation.11 | convolution fusion | flops 553648128 | bytes 4210688 | tf_op jit(solution)/shard_map/nxcd,xdf->nxcf/dot_general | solution.py:165
  233.7 5.2 %fusion.6 = bf16[16,12,2048]{2,0,1:T(8,128)(2,1)} fusion(bf16[1,704,2048]{2,1,0:T(8,128)(2,1)S(1)} %copy-done, bf16[1,2048,704]{1,2,0:T(8,128)(2,1)} %param.38, f32[16,1,12,704]{3,0,2,1:T(8,128)} %fusion.9, bf16[16,12,2048]{2,1,0:T(8,128)(2,1)} %copy-done.4), kind=kOutput, calls=%fused_computation.7 | convolution fusion | flops 1108500480 | bytes 7880704 | tf_op jit(solution)/shard_map/nxcf,xfd->nxcd/dot_general | solution.py:172
  238.9 17.9 %all-reduce.5.cloned.1.call-done = bf16[16,12,2048]{2,0,1:T(8,128)(2,1)} async-done(((bf16[16,12,2048]{2,0,1:T(8,128)(2,1)}), bf16[16,12,2048]{2,0,1:T(8,128)(2,1)}) %all-reduce.5.cloned.1.call-update) | async-done | bytes 786448 | tf_op jit(solution)/shard_map/psum | solution.py:175
  256.8 2.6 copy.65
  259.4 7.1 %all-to-all-start.2 = ((bf16[16,12,2048]{2,1,0:T(8,128)(2,1)}), bf16[16,12,2048]{2,1,0:T(8,128)(2,1)}, u32[]{:S(2)}, u32[]{:S(2)}) async-start(bf16[16,12,2048]{2,1,0:T(8,128)(2,1)} %copy.65), calls=%async_computation.3 | async-start | bytes 2097152 | tf_op jit(solution)/shard_map/all_to_all | solution.py:177
  267.4 25.1 %all-to-all-done.2 = bf16[16,12,2048]{2,1,0:T(8,128)(2,1)} async-done(((bf16[16,12,2048]{2,1,0:T(8,128)(2,1)}), bf16[16,12,2048]{2,1,0:T(8,128)(2,1)}, u32[]{:S(2)}, u32[]{:S(2)}) %all-to-all-start.2) | async-done | bytes 786464 | tf_op jit(solution)/shard_map/all_to_all | solution.py:177
  292.4 2.1 reshape.169
  294.6 1.5 fusion.18
  296.1 0.7 fusion.43
  (97 shorter events, 16.3 us)
Async XLA Ops:
  7.2 226.5 %copy-start = (bf16[1,704,2048]{2,1,0:T(8,128)(2,1)S(1)}, bf16[1,704,2048]{2,1,0:T(8,128)(2,1)}, u32[]{:S(2)}) copy-start(bf16[1,704,2048]{2,1,0:T(8,128)(2,1)} %param.39) | copy-start | bytes 8650756
  10.1 13.8 %all-to-all-start = ((bf16[32,16,128]{2,0,1:T(8,128)(2,1)}), bf16[32,16,128]{2,0,1:T(8,128)(2,1)S(1)}, u32[]{:S(2)}, u32[]{:S(2)}) async-start(bf16[32,16,128]{2,0,1:T(8,128)(2,1)} %copy_bitcast_fusion), calls=%async_computation | async-start | bytes 262144 | tf_op jit(solution)/shard_map/all_to_all | solution.py:104
  17.3 137.1 %reduce-scatter.2.cloned.1.call-start = ((), (), s32[]{:S(2)}) async-start(), calls=%async_computation.4 | async-start | bytes 2506752 | tf_op jit(solution)/shard_map/reduce_scatter | solution.py:106
  18.9 6.9 %copy-start.6 = (bf16[256,128]{1,0:T(8,128)(2,1)S(1)}, bf16[256,128]{1,0:T(8,128)(2,1)}, u32[]{:S(2)}) copy-start(bf16[256,128]{1,0:T(8,128)(2,1)} %param.32) | copy-start | bytes 196612
  20.0 7.9 %copy-start.14 = (f32[32,4]{0,1:T(4,128)S(1)}, f32[32,4]{0,1:T(4,128)}, u32[]{:S(2)}) copy-start(f32[32,4]{0,1:T(4,128)} %param.35) | copy-start | bytes 1540
  20.0 8.0 %copy-start.8 = (s32[32,3]{0,1:T(4,128)S(1)}, s32[32,3]{0,1:T(4,128)}, u32[]{:S(2)}) copy-start(s32[32,3]{0,1:T(4,128)} %param.40) | copy-start | bytes 1156
  25.7 129.9 %copy-start.11 = (f32[4]{0:T(128)S(1)}, f32[4]{0:T(128)}, u32[]{:S(2)}) copy-start(f32[4]{0:T(128)} %param.30) | copy-start | bytes 52
  25.7 129.9 %copy-start.16 = (f32[4]{0:T(128)S(1)}, f32[4]{0:T(128)}, u32[]{:S(2)}) copy-start(f32[4]{0:T(128)} %param.29) | copy-start | bytes 52
  25.8 131.6 %copy-start.5 = (f32[32,4,64]{2,1,0:T(4,128)S(1)}, f32[32,4,64]{2,1,0:T(4,128)}, u32[]{:S(2)}) copy-start(f32[32,4,64]{2,1,0:T(4,128)} %param.34) | copy-start | bytes 98308
  25.8 162.0 %all-reduce.3.cloned.1.call-start = ((), (), s32[]{:S(2)}) async-start(), calls=%async_computation.5 | async-start | bytes 262144 | tf_op jit(solution)/shard_map/psum | solution.py:139
  25.8 4.6 %collective-permute-start.1 = (bf16[256,128]{1,0:T(8,128)(2,1)S(1)}, bf16[256,128]{1,0:T(8,128)(2,1)S(1)}, u32[]{:S(2)}, u32[]{:S(2)}) collective-permute-start(bf16[256,128]{1,0:T(8,128)(2,1)S(1)} %copy-done.6), channel_id=1, source_target_pairs={{0,30},{2,0},{4,2},{6,4},{8,6},{10,8},{12,10},{14,12},{16,14},{18,... | collective-permute-start | bytes 196616 | tf_op jit(solution)/shard_map/ppermute | solution.py:20
  27.4 6.3 %collective-permute-start = (bf16[256,128]{1,0:T(8,128)(2,1)S(1)}, bf16[256,128]{1,0:T(8,128)(2,1)S(1)}, u32[]{:S(2)}, u32[]{:S(2)}) collective-permute-start(bf16[256,128]{1,0:T(8,128)(2,1)S(1)} %copy-done.6), channel_id=1, source_target_pairs={{0,2},{2,4},{4,6},{6,8},{8,10},{10,12},{12,14},{14,16},{16,18},{18... | collective-permute-start | bytes 196616 | tf_op jit(solution)/shard_map/ppermute | solution.py:15
  28.7 141.6 %copy-start.12 = (s32[96]{0:T(128)}, s32[96]{0:T(128)S(1)}, u32[]{:S(2)}) copy-start(s32[96]{0:T(128)S(1)} %select_reduce_fusion) | copy-start | bytes 1156
  30.4 5.3 %collective-permute-start.3 = (bf16[256,128]{1,0:T(8,128)(2,1)S(1)}, bf16[256,128]{1,0:T(8,128)(2,1)S(1)}, u32[]{:S(2)}, u32[]{:S(2)}) collective-permute-start(bf16[256,128]{1,0:T(8,128)(2,1)S(1)} %collective-permute-done.1), channel_id=1, source_target_pairs={{0,30},{2,0},{4,2},{6,4},{8,6},{10,8},{12,10},{14,12},{16,14},{18,... | collective-permute-start | bytes 196616 | tf_op jit(solution)/shard_map/ppermute | solution.py:20
  33.7 6.2 %collective-permute-start.2 = (bf16[256,128]{1,0:T(8,128)(2,1)S(1)}, bf16[256,128]{1,0:T(8,128)(2,1)S(1)}, u32[]{:S(2)}, u32[]{:S(2)}) collective-permute-start(bf16[256,128]{1,0:T(8,128)(2,1)S(1)} %collective-permute-done), channel_id=1, source_target_pairs={{0,2},{2,4},{4,6},{6,8},{8,10},{10,12},{12,14},{14,16},{16,18},{18... | collective-permute-start | bytes 196616 | tf_op jit(solution)/shard_map/ppermute | solution.py:15
  35.8 6.0 %collective-permute-start.5 = (bf16[256,128]{1,0:T(8,128)(2,1)S(1)}, bf16[256,128]{1,0:T(8,128)(2,1)S(1)}, u32[]{:S(2)}, u32[]{:S(2)}) collective-permute-start(bf16[256,128]{1,0:T(8,128)(2,1)S(1)} %collective-permute-done.3), channel_id=1, source_target_pairs={{0,30},{2,0},{4,2},{6,4},{8,6},{10,8},{12,10},{14,12},{16,14},{18,... | collective-permute-start | bytes 196616 | tf_op jit(solution)/shard_map/ppermute | solution.py:20
  39.9 6.6 %collective-permute-start.4 = (bf16[256,128]{1,0:T(8,128)(2,1)S(1)}, bf16[256,128]{1,0:T(8,128)(2,1)S(1)}, u32[]{:S(2)}, u32[]{:S(2)}) collective-permute-start(bf16[256,128]{1,0:T(8,128)(2,1)S(1)} %collective-permute-done.2), channel_id=1, source_target_pairs={{0,2},{2,4},{4,6},{6,8},{8,10},{10,12},{12,14},{14,16},{16,18},{18... | collective-permute-start | bytes 196616 | tf_op jit(solution)/shard_map/ppermute | solution.py:15
  41.8 6.8 %collective-permute-start.7 = (bf16[256,128]{1,0:T(8,128)(2,1)S(1)}, bf16[256,128]{1,0:T(8,128)(2,1)S(1)}, u32[]{:S(2)}, u32[]{:S(2)}) collective-permute-start(bf16[256,128]{1,0:T(8,128)(2,1)S(1)} %collective-permute-done.5), channel_id=1, source_target_pairs={{0,30},{2,0},{4,2},{6,4},{8,6},{10,8},{12,10},{14,12},{16,14},{18,... | collective-permute-start | bytes 196616 | tf_op jit(solution)/shard_map/ppermute | solution.py:20
  46.5 7.0 %collective-permute-start.6 = (bf16[256,128]{1,0:T(8,128)(2,1)S(1)}, bf16[256,128]{1,0:T(8,128)(2,1)S(1)}, u32[]{:S(2)}, u32[]{:S(2)}) collective-permute-start(bf16[256,128]{1,0:T(8,128)(2,1)S(1)} %collective-permute-done.4), channel_id=1, source_target_pairs={{0,2},{2,4},{4,6},{6,8},{8,10},{10,12},{12,14},{14,16},{16,18},{18... | collective-permute-start | bytes 196616 | tf_op jit(solution)/shard_map/ppermute | solution.py:15
  48.6 6.6 %collective-permute-start.9 = (bf16[256,128]{1,0:T(8,128)(2,1)S(1)}, bf16[256,128]{1,0:T(8,128)(2,1)S(1)}, u32[]{:S(2)}, u32[]{:S(2)}) collective-permute-start(bf16[256,128]{1,0:T(8,128)(2,1)S(1)} %collective-permute-done.7), channel_id=1, source_target_pairs={{0,30},{2,0},{4,2},{6,4},{8,6},{10,8},{12,10},{14,12},{16,14},{18,... | collective-permute-start | bytes 196616 | tf_op jit(solution)/shard_map/ppermute | solution.py:20
  53.5 6.4 %collective-permute-start.8 = (bf16[256,128]{1,0:T(8,128)(2,1)S(1)}, bf16[256,128]{1,0:T(8,128)(2,1)S(1)}, u32[]{:S(2)}, u32[]{:S(2)}) collective-permute-start(bf16[256,128]{1,0:T(8,128)(2,1)S(1)} %collective-permute-done.6), channel_id=1, source_target_pairs={{0,2},{2,4},{4,6},{6,8},{8,10},{10,12},{12,14},{14,16},{16,18},{18... | collective-permute-start | bytes 196616 | tf_op jit(solution)/shard_map/ppermute | solution.py:15
  55.2 6.3 %collective-permute-start.11 = (bf16[256,128]{1,0:T(8,128)(2,1)S(1)}, bf16[256,128]{1,0:T(8,128)(2,1)S(1)}, u32[]{:S(2)}, u32[]{:S(2)}) collective-permute-start(bf16[256,128]{1,0:T(8,128)(2,1)S(1)} %collective-permute-done.9), channel_id=1, source_target_pairs={{0,30},{2,0},{4,2},{6,4},{8,6},{10,8},{12,10},{14,12},{16,14},{18,... | collective-permute-start | bytes 196616 | tf_op jit(solution)/shard_map/ppermute | solution.py:20
  59.9 6.5 %collective-permute-start.10 = (bf16[256,128]{1,0:T(8,128)(2,1)S(1)}, bf16[256,128]{1,0:T(8,128)(2,1)S(1)}, u32[]{:S(2)}, u32[]{:S(2)}) collective-permute-start(bf16[256,128]{1,0:T(8,128)(2,1)S(1)} %collective-permute-done.8), channel_id=1, source_target_pairs={{0,2},{2,4},{4,6},{6,8},{8,10},{10,12},{12,14},{14,16},{16,18},{18... | collective-permute-start | bytes 196616 | tf_op jit(solution)/shard_map/ppermute | solution.py:15
  61.5 11.9 %collective-permute-start.13 = (bf16[256,128]{1,0:T(8,128)(2,1)S(1)}, bf16[256,128]{1,0:T(8,128)(2,1)S(1)}, u32[]{:S(2)}, u32[]{:S(2)}) collective-permute-start(bf16[256,128]{1,0:T(8,128)(2,1)S(1)} %collective-permute-done.11), channel_id=1, source_target_pairs={{0,30},{2,0},{4,2},{6,4},{8,6},{10,8},{12,10},{14,12},{16,14},{18,... | collective-permute-start | bytes 196616 | tf_op jit(solution)/shard_map/ppermute | solution.py:20
  66.4 6.4 %collective-permute-start.12 = (bf16[256,128]{1,0:T(8,128)(2,1)S(1)}, bf16[256,128]{1,0:T(8,128)(2,1)S(1)}, u32[]{:S(2)}, u32[]{:S(2)}) collective-permute-start(bf16[256,128]{1,0:T(8,128)(2,1)S(1)} %collective-permute-done.10), channel_id=1, source_target_pairs={{0,2},{2,4},{4,6},{6,8},{8,10},{10,12},{12,14},{14,16},{16,18},{18... | collective-permute-start | bytes 196616 | tf_op jit(solution)/shard_map/ppermute | solution.py:15
  72.8 6.1 %collective-permute-start.14 = (bf16[256,128]{1,0:T(8,128)(2,1)S(1)}, bf16[256,128]{1,0:T(8,128)(2,1)S(1)}, u32[]{:S(2)}, u32[]{:S(2)}) collective-permute-start(bf16[256,128]{1,0:T(8,128)(2,1)S(1)} %collective-permute-done.12), channel_id=1, source_target_pairs={{0,2},{2,4},{4,6},{6,8},{8,10},{10,12},{12,14},{14,16},{16,18},{18... | collective-permute-start | bytes 196616 | tf_op jit(solution)/shard_map/ppermute | solution.py:15
  162.0 2.0 copy-start.1
  164.0 4.0 %copy-start.15 = (f32[256]{0:T(256)S(1)}, f32[256]{0:T(256)}, u32[]{:S(2)}) copy-start(f32[256]{0:T(256)} %param.31) | copy-start | bytes 3076
  164.0 23.8 %copy-start.2 = (bf16[32,2048]{1,0:T(8,128)(2,1)S(1)}, bf16[32,2048]{1,0:T(8,128)(2,1)}, u32[]{:S(2)}) copy-start(bf16[32,2048]{1,0:T(8,128)(2,1)} %param.21) | copy-start | bytes 393220
  164.0 24.9 %copy-start.7 = (f32[2048]{0:T(1024)S(1)}, f32[2048]{0:T(1024)}, u32[]{:S(2)}) copy-start(f32[2048]{0:T(1024)} %param.36) | copy-start | bytes 24580
  170.2 86.6 %all-reduce.5.cloned.1.call-start = ((), (), s32[]{:S(2)}) async-start(), calls=%async_computation.6 | async-start | bytes 1572864 | tf_op jit(solution)/shard_map/psum | solution.py:175
  228.9 1.0 copy-start.4
  238.9 27.6 %copy-start.13 = (s32[96]{0:T(128)S(1)}, s32[96]{0:T(128)}, u32[]{:S(2)}) copy-start(s32[96]{0:T(128)} %copy-done.12) | copy-start | bytes 1156
  238.9 27.8 %copy-start.9 = (s32[32,3]{0,1:T(4,128)S(1)}, s32[32,3]{0,1:T(4,128)}, u32[]{:S(2)}) copy-start(s32[32,3]{0,1:T(4,128)} %param.40) | copy-start | bytes 1156
  238.9 55.7 %copy-start.10 = (f32[32,3]{0,1:T(4,128)S(1)}, f32[32,3]{0,1:T(4,128)}, u32[]{:S(2)}) copy-start(f32[32,3]{0,1:T(4,128)} %param.41) | copy-start | bytes 1156
  259.4 36.7 %copy-start.3 = (bf16[32,2048]{1,0:T(8,128)(2,1)S(1)}, bf16[32,2048]{1,0:T(8,128)(2,1)}, u32[]{:S(2)}) copy-start(bf16[32,2048]{1,0:T(8,128)(2,1)} %all-reduce.3.cloned.1.call-done) | copy-start | bytes 393220
  259.4 33.0 %all-to-all-start.2 = ((bf16[16,12,2048]{2,1,0:T(8,128)(2,1)}), bf16[16,12,2048]{2,1,0:T(8,128)(2,1)}, u32[]{:S(2)}, u32[]{:S(2)}) async-start(bf16[16,12,2048]{2,1,0:T(8,128)(2,1)} %copy.65), calls=%async_computation.3 | async-start | bytes 2097152 | tf_op jit(solution)/shard_map/all_to_all | solution.py:177
Sparse Core Ops, SparseCore 0:
  25.9 128.3 reduce-scatter.1
  170.3 17.4 all-reduce.2
  239.0 17.7 all-reduce.4
